TPU v7x, 512 devices: a whole 4x8x8 slice. The times are simulated.
512 devices in a mesh: ep: 32 (over z, x), tp: 16 (over y, core).
Axes of the slice: x: 4, y: 8, z: 8, core: 2. Of those that a mesh axis runs over, the one named last changes fastest.
Arguments:
- queries: bfloat16 [4096, 512], P('ep'), may hold values from -6 to 6
- key_vectors: bfloat16 [4096, 512], P('ep'), may hold values from -6 to 6
- values: bfloat16 [4096, 1024], P('ep', 'tp'), may hold values from -6 to 6
- out_gate: bfloat16 [4096, 1024], P('ep', 'tp'), may hold values from -6 to 6
- input_gate: float32 [4096, 2], P('ep'), may hold values from -8 to 130
- forget_gate: float32 [4096, 2], P('ep'), may hold values from -2 to 16
- mix_weight: bfloat16 [1024, 2048], P('tp'), may hold values from -0.1875 to 0.1875
- expert_input: bfloat16 [8192, 2048], P('ep'), may hold values from -6 to 6
- norm_gain: float32 [2048], replicated, may hold values from 0.1 to 1.9
- route_ids: int32 [8192, 4], P('ep'), may hold values from 0 to 63, all different within a row; in each aligned block of 256 rows (0 to 255, 256 to 511, ...) at most 32 rows name the same one
- route_weights: float32 [8192, 4], P('ep'), may hold values from 0.2 to 1.2
- expert_gate: bfloat16 [512, 2048, 128], P(('ep', 'tp')), may hold values from -0.125 to 0.125
- expert_up: bfloat16 [512, 2048, 128], P(('ep', 'tp')), may hold values from -0.125 to 0.125
- expert_down: bfloat16 [512, 128, 2048], P(('ep', 'tp')), may hold values from -0.1875 to 0.1875
- shared_gate: bfloat16 [2048, 512], P(None, 'tp'), may hold values from -0.125 to 0.125
- shared_up: bfloat16 [2048, 512], P(None, 'tp'), may hold values from -0.125 to 0.125
- shared_down: bfloat16 [512, 2048], P('tp'), may hold values from -0.25 to 0.25
Outputs:
- mixer_out: bfloat16 [4096, 2048], P('ep')
- expert_out: bfloat16 [8192, 2048], P('ep')
Inputs may be any that keep to these rules, and one draw needn't show every extreme that they name: `route_ids`: each row names 4 different experts. In each aligned block of 256 rows (the rows of one index of ep) no expert is named by more than 32 rows, and in some block one expert is named by exactly 32 rows.
All inputs are finite; a program needn't handle non-finite values.
Results may differ from a plain program's by a relative error of at most 0.01575.
Values may be sent and summed in bfloat16 or wider, within the bound.
A program may use at most 64 MiB of HBM per device.

v0:
```python
import jax
import jax.numpy as jnp
from jax import lax
from jax.sharding import Mesh
from jax.sharding import PartitionSpec as P

D = 2048
MEMORY_HEADS = 2
KEY_DIM = 256
BLOCK = 128
FF = 1024
EP = ("ep_0", "ep_1")
EP_TP = ("ep_0", "ep_1", "tp")
epsilon = 1e-06
lowest = -1e30
den_floor = 4.0


def nothing_yet(array, identity):
    return jax.tree.map(
        lambda part, zero: jnp.zeros_like(part) + jnp.asarray(zero, part.dtype), array, identity
    )


def all_in_one(array, axis):
    leaves = jax.tree.leaves(array)
    order = sorted(range(len(leaves)), key=lambda k: -leaves[k].size)
    width = (1, *leaves[order[0]].shape)[-1]
    lines = [
        jnp.pad(leaves[k].reshape(-1), (0, -leaves[k].size % width)).reshape(-1, width)
        for k in order
    ]
    both, at, found = (lax.all_gather(jnp.concatenate(lines), axis), 0, {})
    for k, line in zip(order, lines):
        section = both[:, at : at + len(line)].reshape(len(both), -1)
        found[k] = section[:, : leaves[k].size].reshape(-1, *leaves[k].shape)
        at += len(line)
    numbers = iter(range(len(leaves)))
    return jax.tree.map(lambda _: found[next(numbers)], array)


def entering_2(array, axes, combine, identity):
    before = start = nothing_yet(array, identity)
    subtotal = array
    for axis in reversed(axes):
        count, place = (lax.axis_size(axis), lax.axis_index(axis))
        pieces = all_in_one(subtotal, axis)
        inside, subtotal = (start, start)
        for k in range(count):
            passed = k < place
            subtotal = combine(subtotal, jax.tree.map(lambda part: part[k], pieces))
            inside = jax.tree.map(lambda new, old: jnp.where(passed, new, old), subtotal, inside)
        before = combine(inside, before)
    return before


def in_blocks(array, dim, count):
    before, after = (array.shape[:dim], array.shape[dim + 1 :])
    return jnp.moveaxis(array.reshape(*before, count, -1, *after), dim, 0)


def summed_on_arrival(array, axis, dim):
    blocks = in_blocks(array, dim, lax.axis_size(axis))
    arrived = lax.all_to_all(blocks, axis, split_axis=0, concat_axis=0, tiled=True)
    return arrived.astype(jnp.float32).sum(axis=0)


def from_everyone(array, axis):
    copies = jnp.broadcast_to(array, (lax.axis_size(axis), *array.shape))
    return lax.all_to_all(copies, axis, split_axis=0, concat_axis=0, tiled=True)


def in_order(blocks, dim):
    blocks = jnp.moveaxis(blocks, 0, dim)
    shape = blocks.shape
    return blocks.reshape(*shape[:dim], shape[dim] * shape[dim + 1], *shape[dim + 2 :])


def collect(array, axis, dim):
    blocks = from_everyone(array, axis)
    return in_order(blocks, dim)


def combine_segments(earlier, later):
    first_decay, first_memory, first_normalizer, first_running = earlier
    second_decay, second_memory, second_normalizer, second_running = later
    running = jnp.maximum(second_decay + first_running, second_running)
    lead_scale = jnp.exp(second_decay + first_running - running)
    tail_scale = jnp.exp(second_running - running)
    return (
        first_decay + second_decay,
        lead_scale * first_memory + tail_scale * second_memory,
        lead_scale * first_normalizer + tail_scale * second_normalizer,
        running,
    )


def mixer_half(queries, key_vectors, values, out_gate, input_gate, forget_gate, mix_weight):
    tp_count = lax.axis_size("tp")
    tp_rank = lax.axis_index("tp")
    length = queries.shape[0]
    blocks = length // BLOCK
    channels = values.shape[1]
    factor = KEY_DIM ** (-0.5)
    head_index = tp_rank // (tp_count // MEMORY_HEADS)
    offset = head_index * KEY_DIM
    query_head = lax.dynamic_slice_in_dim(queries, offset, KEY_DIM, 1).reshape(
        blocks, BLOCK, KEY_DIM
    )
    key_head = lax.dynamic_slice_in_dim(key_vectors, offset, KEY_DIM, 1).reshape(
        blocks, BLOCK, KEY_DIM
    )
    value_blocks = values.reshape(blocks, BLOCK, channels)
    select = jnp.arange(MEMORY_HEADS, dtype=jnp.int32)[None, :] == head_index
    input_head = jnp.sum(jnp.where(select, input_gate, 0.0), axis=1).reshape(blocks, BLOCK)
    forget_head = jax.nn.log_sigmoid(jnp.sum(jnp.where(select, forget_gate, 0.0), axis=1)).reshape(
        blocks, BLOCK
    )
    cumulative = jnp.cumsum(forget_head, axis=1)
    block_total = cumulative[:, -1]
    log_retention = block_total[:, None] - cumulative + input_head
    block_running = jnp.max(log_retention, axis=1)
    weighted_keys = (
        key_head.astype(jnp.float32) * jnp.exp(log_retention - block_running[:, None])[:, :, None]
    )
    block_memory = jnp.einsum(
        "bsd,bsv->bdv",
        weighted_keys,
        value_blocks.astype(jnp.float32),
        precision=lax.Precision.HIGHEST,
    )
    block_normalizer = jnp.sum(weighted_keys, axis=1)
    segments = (block_total, block_memory, block_normalizer, block_running)
    neutral = (
        jnp.zeros((), jnp.float32),
        jnp.zeros((KEY_DIM, channels), jnp.float32),
        jnp.zeros((KEY_DIM,), jnp.float32),
        jnp.full((), lowest, jnp.float32),
    )

    def fold_block(carry_in, segment):
        return (combine_segments(carry_in, segment), None)

    summary, _ = lax.scan(fold_block, neutral, segments)
    prefix = entering_2(summary, EP, combine_segments, neutral)
    start_state = (
        jnp.zeros((), jnp.float32),
        jnp.zeros((KEY_DIM, channels), jnp.float32),
        jnp.zeros((KEY_DIM,), jnp.float32),
        jnp.zeros((), jnp.float32),
    )
    entering = combine_segments(start_state, prefix)
    causal = jnp.tril(jnp.ones((BLOCK, BLOCK), dtype=bool))

    def block_pass(carry_in, inputs):
        query_block, key_block, value_block, input_block, cumulative_block, segment = inputs
        _, memory, normalizer, running = carry_in
        carried = cumulative_block + running
        log_weight = cumulative_block[:, None] - cumulative_block[None, :] + input_block[None, :]
        log_weight = jnp.where(causal, log_weight, -jnp.inf)
        stabilizer = jnp.maximum(carried, jnp.max(log_weight, axis=1))
        within = jnp.exp(log_weight - stabilizer[:, None])
        across = jnp.exp(carried - stabilizer)
        scores = (
            jnp.einsum("td,sd->ts", query_block, key_block, preferred_element_type=jnp.float32)
            * factor
        )
        weights = scores * within
        scaled = query_block.astype(jnp.float32) * factor
        numerator = across[:, None] * jnp.dot(scaled, memory, precision=lax.Precision.HIGHEST)
        numerator = numerator + jnp.dot(
            weights.astype(jnp.bfloat16), value_block, preferred_element_type=jnp.float32
        )
        denominator = across * jnp.dot(scaled, normalizer, precision=lax.Precision.HIGHEST)
        denominator = denominator + jnp.sum(weights, axis=1)
        hidden = numerator / jnp.maximum(jnp.abs(denominator), den_floor)[:, None]
        return (combine_segments(carry_in, segment), hidden)

    _, hidden = lax.scan(
        block_pass, entering, (query_head, key_head, value_blocks, input_head, cumulative, segments)
    )
    gated_rows = (
        hidden.reshape(length, channels) * jax.nn.sigmoid(out_gate.astype(jnp.float32))
    ).astype(jnp.bfloat16)
    return jnp.dot(gated_rows, mix_weight, preferred_element_type=jnp.float32)


def expert_half(
    expert_input,
    norm_gain,
    route_ids,
    route_weights,
    expert_gate,
    expert_up,
    expert_down,
    shared_gate,
    shared_up,
    shared_down,
):
    ep_count = lax.axis_size(EP)
    tp_count = lax.axis_size("tp")
    tp_rank = lax.axis_index("tp")
    tokens = expert_input.shape[0]
    top_count = route_ids.shape[1]
    slice_units = expert_gate.shape[2]
    group_size = FF // slice_units
    per_ep = tp_count // group_size
    team_index = tp_rank // group_size
    expert_count = ep_count * per_ep
    capacity = 2 * tokens * top_count // expert_count
    rows_wide = expert_input.astype(jnp.float32)
    normed = (
        rows_wide
        * lax.rsqrt(jnp.mean(rows_wide * rows_wide, axis=-1, keepdims=True) + epsilon)
        * norm_gain
    ).astype(jnp.bfloat16)
    chosen = route_ids.reshape(-1)
    onehot = (chosen[:, None] == jnp.arange(expert_count, dtype=jnp.int32)[None, :]).astype(
        jnp.int32
    )
    slot_rank = jnp.sum((jnp.cumsum(onehot, axis=0) - onehot) * onehot, axis=1)
    in_team = chosen % per_ep == team_index
    target = jnp.where(in_team, chosen // per_ep * capacity + slot_rank, ep_count * capacity)
    token_of = jnp.arange(chosen.shape[0], dtype=jnp.int32) // top_count
    slot_token = jnp.zeros((ep_count * capacity,), jnp.int32).at[target].set(token_of, mode="drop")
    slot_live = jnp.zeros((ep_count * capacity,), jnp.int32).at[target].set(1, mode="drop")
    outgoing = jnp.where(slot_live[:, None] > 0, normed[slot_token], jnp.zeros((), jnp.bfloat16))
    outgoing = outgoing.reshape(ep_count, capacity, D)
    gate_slice = expert_gate[0]
    up_slice = expert_up[0]
    down_slice = expert_down[0]
    arrived = lax.all_to_all(outgoing, EP, split_axis=0, concat_axis=0, tiled=True)
    gate_val = jnp.einsum("sid,df->sif", arrived, gate_slice, preferred_element_type=jnp.float32)
    up_val = jnp.einsum("sid,df->sif", arrived, up_slice, preferred_element_type=jnp.float32)
    hidden = (jax.nn.silu(gate_val) * up_val).astype(jnp.bfloat16)
    partial_value = jnp.einsum(
        "sif,fd->sid", hidden, down_slice, preferred_element_type=jnp.float32
    )
    partial_value = partial_value.astype(jnp.bfloat16)
    returned = lax.all_to_all(partial_value, EP, split_axis=0, concat_axis=0, tiled=True)
    flat_back = returned.reshape(ep_count * capacity, returned.shape[2])
    gather_at = jnp.where(in_team, target, 0).reshape(tokens, top_count)
    weight_at = jnp.where(in_team, route_weights.reshape(-1), 0.0).reshape(tokens, top_count)
    combined = jnp.zeros((tokens, returned.shape[2]), jnp.float32)
    for pick_index in range(top_count):
        combined = (
            combined
            + flat_back[gather_at[:, pick_index]].astype(jnp.float32)
            * weight_at[:, pick_index][:, None]
        )
    shared_gate_val = jnp.dot(normed, shared_gate, preferred_element_type=jnp.float32)
    shared_up_val = jnp.dot(normed, shared_up, preferred_element_type=jnp.float32)
    shared_act = (jax.nn.silu(shared_gate_val) * shared_up_val).astype(jnp.bfloat16)
    return combined + jnp.dot(shared_act, shared_down, preferred_element_type=jnp.float32)


def shards(
    queries,
    key_vectors,
    values,
    out_gate,
    input_gate,
    forget_gate,
    mix_weight,
    expert_input,
    norm_gain,
    route_ids,
    route_weights,
    expert_gate,
    expert_up,
    expert_down,
    shared_gate,
    shared_up,
    shared_down,
):
    mixer_partial = mixer_half(
        queries, key_vectors, values, out_gate, input_gate, forget_gate, mix_weight
    )
    expert_partial = expert_half(
        expert_input,
        norm_gain,
        route_ids,
        route_weights,
        expert_gate,
        expert_up,
        expert_down,
        shared_gate,
        shared_up,
        shared_down,
    )
    mixer_piece = summed_on_arrival(mixer_partial.astype(jnp.bfloat16), "tp", 0).astype(
        jnp.bfloat16
    )
    mixer_out = lax.all_gather(mixer_piece, "tp", axis=0, tiled=True)
    expert_piece = lax.psum_scatter(expert_partial, "tp", scatter_dimension=0, tiled=True).astype(
        jnp.bfloat16
    )
    expert_out = collect(expert_piece, "tp", 0)
    return (mixer_out, expert_out)


def solution(mesh):
    finer = Mesh(mesh.devices.reshape(8, 4, mesh.shape["tp"]), ("ep_0", "ep_1", "tp"))
    placed = (
        P(EP, None),
        P(EP, None),
        P(EP, "tp"),
        P(EP, "tp"),
        P(EP, None),
        P(EP, None),
        P("tp", None),
        P(EP, None),
        P(),
        P(EP, None),
        P(EP, None),
        P(EP_TP, None, None),
        P(EP_TP, None, None),
        P(EP_TP, None, None),
        P(None, "tp"),
        P(None, "tp"),
        P("tp", None),
    )
    return jax.shard_map(
        shards, mesh=finer, in_specs=placed, out_specs=(P(EP, None), P(EP, None)), check_vma=False
    )
```

profile of v0, /device:TPU:1, one launch (start us, length us, event | category | flops | bytes accessed | tf_op | source)
XLA Modules:
  0.0 426.6 jit_solution(15270256443497055373)
XLA Ops:
  7.2 0.9 copy.108
  8.6 18.0 %reduce-window.6 = s32[64,8,128]{2,1,0:T(8,128)S(1)} reduce-window(s32[64,8,128]{2,1,0:T(8,128)S(1)} %fusion.29, s32[]{:T(128)} %constant.140.clone.1), window={size=1x1x128 pad=0_0x0_0x127_0}, to_apply=%region_8.9 | reduce-window | flops 8323072 | bytes 524292 | tf_op jit(solution)/shard_map/reduce-window
  27.3 4.3 %scatter_custom_fusion.1 = s32[1024]{0:T(1024)S(1)} fusion(s32[1024]{0:T(1024)S(1)} %bitcast.173, s32[1024]{0:T(1024)S(1)} %add_select_fusion.3, s32[]{:T(128)} %constant.140.clone.1), kind=kCustom, calls=%fused_computation.234 | custom fusion | bytes 4100 | tf_op jit(solution)/shard_map/scatter | solution.py:225
  31.9 4.3 %scatter_custom_fusion = s32[1024]{0:T(1024)S(1)} fusion(s32[1024]{0:T(1024)S(1)} %bitcast.174, s32[1024]{0:T(1024)S(1)} %broadcast.491, s32[]{:T(128)} %constant.140.clone.1), kind=kCustom, calls=%fused_computation.237 | custom fusion | bytes 4100 | tf_op jit(solution)/shard_map/scatter | solution.py:226
  36.6 6.0 %gather_fusion = bf16[1024,2048]{1,0:T(8,128)(2,1)} fusion(bf16[256,2048]{1,0:T(8,128)(2,1)S(1)} %fusion.3, s32[1024]{0:T(1024)S(1)} %fusion.157), kind=kCustom, calls=%fused_computation | custom fusion | bytes 8392704 | tf_op jit(solution)/shard_map/gather | solution.py:227
  42.7 2.5 broadcast_select_fusion
  45.2 107.2 %all_to_all.20 = bf16[32,32,2048]{2,1,0:T(8,128)(2,1)S(1)} all-to-all(bf16[32,32,2048]{2,1,0:T(8,128)(2,1)S(1)} %broadcast_select_fusion), channel_id=1, replica_groups=mesh['ep_0'=8,'ep_1'=4,'tp'=16] {'ep_0','ep_1'}, dimensions={0} | all-to-all | bytes 8388608 | tf_op jit(solution)/shard_map/all_to_all | solution.py:232
  152.5 1.9 copy-done.1
  154.4 1.2 fusion.18
  155.7 8.5 %convolution_convert_fusion = bf16[32,32,2048]{2,1,0:T(8,128)(2,1)} fusion(bf16[32,32,2048]{2,1,0:T(8,128)(2,1)} %copy-done.1, bf16[1,128,2048]{2,1,0:T(8,128)(2,1)S(1)} %copy-done, bf16[1,2048,128]{2,1,0:T(8,128)(2,1)S(1)} %copy-done.4, f32[32,32,128]{2,1,0:T(8,128)S(1)} %fusion.18), kind=kOutput, calls=%fused_computation.8 | convolution fusion | flops 1076625408 | bytes 9961472 | tf_op jit(solution)/shard_map/sif,fd->sid/dot_general | solution.py:236
  164.2 6.7 %all-to-all-start.2 = ((bf16[32,32,2048]{2,1,0:T(8,128)(2,1)}), bf16[32,32,2048]{2,1,0:T(8,128)(2,1)}, u32[]{:S(2)}, u32[]{:S(2)}) async-start(bf16[32,32,2048]{2,1,0:T(8,128)(2,1)} %convolution_convert_fusion), calls=%async_computation.2 | async-start | bytes 8388608 | tf_op jit(solution)/shard_map/all_to_all | solution.py:240
  172.7 1.2 fusion.178
  175.4 1.3 subtract_exponential_fusion.1
  178.2 20.0 %all-gather.2 = f32[4,262,64]{1,2,0:T(8,128)S(1)} all-gather(f32[1,262,64]{1,2,0:T(8,128)S(1)} %maximum_bitcast_fusion), channel_id=2, replica_groups=mesh['ep_0'=8,'ep_1'=4,'tp'=16] {'ep_1'}, dimensions={0}, use_global_device_ids=true | all-gather | bytes 335360 | tf_op jit(solution)/shard_map/all_gather | solution.py:33
  211.3 0.7 copy.96
  213.8 0.9 slice_reduce_fusion.3
  215.1 48.3 %all-to-all-done.2 = bf16[32,32,2048]{2,1,0:T(8,128)(2,1)} async-done(((bf16[32,32,2048]{2,1,0:T(8,128)(2,1)}), bf16[32,32,2048]{2,1,0:T(8,128)(2,1)}, u32[]{:S(2)}, u32[]{:S(2)}) %all-to-all-start.2) | async-done | bytes 4194336 | tf_op jit(solution)/shard_map/all_to_all | solution.py:240
  263.5 5.2 %gather_fusion.1 = bf16[256,2048]{1,0:T(8,128)(2,1)S(1)} fusion(bf16[1024,2048]{1,0:T(8,128)(2,1)} %bitcast.58, s32[1024]{0:T(1024)} %get-tuple-element.135), kind=kCustom, calls=%fused_computation.1 | custom fusion | bytes 2098176 | tf_op jit(solution)/shard_map/gather | solution.py:248
  268.7 6.2 %gather_fusion.2 = bf16[256,2048]{1,0:T(8,128)(2,1)} fusion(bf16[1024,2048]{1,0:T(8,128)(2,1)} %bitcast.58, s32[1024]{0:T(1024)} %get-tuple-element.134), kind=kCustom, calls=%fused_computation.2 | custom fusion | bytes 2098176 | tf_op jit(solution)/shard_map/gather | solution.py:248
  274.9 6.2 %gather_fusion.3 = bf16[256,2048]{1,0:T(8,128)(2,1)} fusion(bf16[1024,2048]{1,0:T(8,128)(2,1)} %bitcast.58, s32[1024]{0:T(1024)} %get-tuple-element.133), kind=kCustom, calls=%fused_computation.3 | custom fusion | bytes 2098176 | tf_op jit(solution)/shard_map/gather | solution.py:248
  281.2 6.2 %gather_fusion.4 = bf16[256,2048]{1,0:T(8,128)(2,1)} fusion(bf16[1024,2048]{1,0:T(8,128)(2,1)} %bitcast.58, s32[1024]{0:T(1024)} %get-tuple-element.132), kind=kCustom, calls=%fused_computation.4 | custom fusion | bytes 2098176 | tf_op jit(solution)/shard_map/gather | solution.py:248
  287.4 5.0 %convolution_add_fusion = f32[256,2048]{1,0:T(8,128)} fusion(bf16[32,2048]{1,0:T(8,128)(2,1)S(1)} %copy-done.6, bf16[256,2048]{1,0:T(8,128)(2,1)} %gather_fusion.4, bf16[256,2048]{1,0:T(8,128)(2,1)} %gather_fusion.3, bf16[256,2048]{1,0:T(8,128)(2,1)} %gather_fusion.2, bf16[256,2048]{1,0:T(8,128)(2,1)S(1)} %gather_fusion.1, bf16[256,2048]{1,0:T(8,128)(2,1)S(1)} %fusion.3, ...), kind=kOutput, calls=%fused_computation.9 | convolution fusion | flops 73449472 | bytes 7639040 | tf_op jit(solution)/shard_map/dot_general | solution.py:254
  293.3 21.1 %all-gather.3 = f32[8,262,64]{1,2,0:T(8,128)S(1)} all-gather(f32[1,262,64]{1,2,0:T(8,128)S(1)} %maximum_bitcast_fusion.1), channel_id=3, replica_groups=mesh['ep_0'=8,'ep_1'=4,'tp'=16] {'ep_0'}, dimensions={0}, use_global_device_ids=true | all-gather | bytes 603648 | tf_op jit(solution)/shard_map/all_gather | solution.py:33
  340.8 1.3 fusion
  342.1 16.0 %all-to-all-start = ((bf16[16,8,2048]{2,1,0:T(8,128)(2,1)}), bf16[16,8,2048]{2,1,0:T(8,128)(2,1)S(1)}, u32[]{:S(2)}, u32[]{:S(2)}) async-start(bf16[16,8,2048]{2,1,0:T(8,128)(2,1)} %fusion), calls=%async_computation | async-start | bytes 1048576 | tf_op jit(solution)/shard_map/all_to_all | solution.py:64
  358.1 0.9 convert_element_type.83
  359.0 16.3 %all-to-all-done = bf16[16,8,2048]{2,1,0:T(8,128)(2,1)S(1)} async-done(((bf16[16,8,2048]{2,1,0:T(8,128)(2,1)}), bf16[16,8,2048]{2,1,0:T(8,128)(2,1)S(1)}, u32[]{:S(2)}, u32[]{:S(2)}) %all-to-all-start) | async-done | bytes 524320 | tf_op jit(solution)/shard_map/all_to_all | solution.py:64
  375.3 1.1 broadcast_in_dim.93
  376.4 3.6 all-to-all-start.3
  380.0 37.9 %all_gather.19 = bf16[128,2048]{1,0:T(8,128)(2,1)S(1)} all-gather(bf16[8,2048]{1,0:T(8,128)(2,1)S(1)} %reduce_sum.75), channel_id=1, replica_groups=mesh['ep_0'=8,'ep_1'=4,'tp'=16] {'tp'}, dimensions={0}, use_global_device_ids=true | all-gather | bytes 557056 | tf_op jit(solution)/shard_map/all_gather | solution.py:294
  418.0 0.8 copy.149
  418.8 1.0 copy.150
  (151 shorter events, 13.9 us)
Async XLA Ops:
  7.2 148.5 %copy-start = (bf16[1,128,2048]{2,1,0:T(8,128)(2,1)S(1)}, bf16[1,128,2048]{2,1,0:T(8,128)(2,1)}, u32[]{:S(2)}) copy-start(bf16[1,128,2048]{2,1,0:T(8,128)(2,1)} %param.30) | copy-start | bytes 1572868
  7.2 24.4 %copy-start.2 = (bf16[256,2048]{1,0:T(8,128)(2,1)S(1)}, bf16[256,2048]{1,0:T(8,128)(2,1)}, u32[]{:S(2)}) copy-start(bf16[256,2048]{1,0:T(8,128)(2,1)} %param.24) | copy-start | bytes 3145732
  7.2 29.1 %copy-start.25 = (f32[2048]{0:T(1024)S(1)}, f32[2048]{0:T(1024)}, u32[]{:S(2)}) copy-start(f32[2048]{0:T(1024)} %param.25) | copy-start | bytes 24580
  45.2 109.2 %copy-start.3 = (bf16[1,2048,128]{2,1,0:T(8,128)(2,1)S(1)}, bf16[1,2048,128]{2,1,0:T(8,128)(2,1)}, u32[]{:S(2)}) copy-start(bf16[1,2048,128]{2,1,0:T(8,128)(2,1)} %param.28) | copy-start | bytes 1572868
  152.5 1.9 copy-start.1
  154.4 1.3 copy-start.4
  164.2 6.9 %copy-start.29 = (f32[128,2]{0,1:T(2,128)S(1)}, f32[128,2]{0,1:T(2,128)}, u32[]{:S(2)}) copy-start(f32[128,2]{0,1:T(2,128)} %param.21) | copy-start | bytes 3076
  164.2 6.9 %copy-start.30 = (f32[128,2]{0,1:T(2,128)S(1)}, f32[128,2]{0,1:T(2,128)}, u32[]{:S(2)}) copy-start(f32[128,2]{0,1:T(2,128)} %param.22) | copy-start | bytes 3076
  164.2 12.5 %copy-start.9 = (bf16[128,512]{1,0:T(8,128)(2,1)S(1)}, bf16[128,512]{1,0:T(8,128)(2,1)}, u32[]{:S(2)}) copy-start(bf16[128,512]{1,0:T(8,128)(2,1)} %param.18) | copy-start | bytes 393220
  164.2 13.7 %copy-start.11 = (bf16[128,64]{0,1:T(8,128)(2,1)S(1)}, bf16[128,64]{0,1:T(8,128)(2,1)}, u32[]{:S(2)}) copy-start(bf16[128,64]{0,1:T(8,128)(2,1)} %param.19) | copy-start | bytes 49156
  164.2 43.6 %copy-start.22 = (s32[256,4]{0,1:T(4,128)S(1)}, s32[256,4]{0,1:T(4,128)}, u32[]{:S(2)}) copy-start(s32[256,4]{0,1:T(4,128)} %param.26) | copy-start | bytes 12292
  164.2 43.8 %copy-start.28 = (f32[256,4]{0,1:T(4,128)S(1)}, f32[256,4]{0,1:T(4,128)}, u32[]{:S(2)}) copy-start(f32[256,4]{0,1:T(4,128)} %param.27) | copy-start | bytes 12292
  164.2 99.3 %all-to-all-start.2 = ((bf16[32,32,2048]{2,1,0:T(8,128)(2,1)}), bf16[32,32,2048]{2,1,0:T(8,128)(2,1)}, u32[]{:S(2)}, u32[]{:S(2)}) async-start(bf16[32,32,2048]{2,1,0:T(8,128)(2,1)} %convolution_convert_fusion), calls=%async_computation.2 | async-start | bytes 8388608 | tf_op jit(solution)/shard_map/all_to_all | solution.py:240
  170.9 187.2 %reduce-scatter.2.cloned.1.call-start = ((), (), s32[]{:S(2)}) async-start(), calls=%async_computation.5 | async-start | bytes 2228224 | tf_op jit(solution)/shard_map/reduce_scatter | solution.py:295
  171.2 5.6 %copy-start.26 = (f32[128]{0:T(128)}, f32[128]{0:T(128)S(1)}, u32[]{:S(2)}) copy-start(f32[128]{0:T(128)S(1)} %get-tuple-element.69) | copy-start | bytes 1540
  171.5 37.0 %copy-start.23 = (f32[1,128]{1,0:T(1,128)}, f32[1,128]{1,0:T(1,128)S(1)}, u32[]{:S(2)}) copy-start(f32[1,128]{1,0:T(1,128)S(1)} %reduce_window_sum.26) | copy-start | bytes 1540
  177.9 36.9 %copy-start.8 = (bf16[2048,32]{0,1:T(8,128)(2,1)S(1)}, bf16[2048,32]{0,1:T(8,128)(2,1)}, u32[]{:S(2)}) copy-start(bf16[2048,32]{0,1:T(8,128)(2,1)} %param.31) | copy-start | bytes 393220
  208.7 0.6 copy-start.15
  281.2 6.2 %copy-start.6 = (bf16[32,2048]{1,0:T(8,128)(2,1)S(1)}, bf16[32,2048]{1,0:T(8,128)(2,1)}, u32[]{:S(2)}) copy-start(bf16[32,2048]{1,0:T(8,128)(2,1)} %param.33) | copy-start | bytes 393220
  281.2 6.2 %copy-start.7 = (bf16[2048,32]{0,1:T(8,128)(2,1)S(1)}, bf16[2048,32]{0,1:T(8,128)(2,1)}, u32[]{:S(2)}) copy-start(bf16[2048,32]{0,1:T(8,128)(2,1)} %param.32) | copy-start | bytes 393220
  292.4 0.8 copy-start.10
  292.5 47.1 %copy-start.14 = (f32[1,4,64]{2,1,0:T(4,128)S(1)}, f32[1,4,64]{2,1,0:T(4,128)}, u32[]{:S(2)}) copy-start(f32[1,4,64]{2,1,0:T(4,128)} %copy-done.13) | copy-start | bytes 3076
  292.5 47.1 %copy-start.16 = (f32[1,4,64]{2,1,0:T(4,128)S(1)}, f32[1,4,64]{2,1,0:T(4,128)}, u32[]{:S(2)}) copy-start(f32[1,4,64]{2,1,0:T(4,128)} %copy-done.15) | copy-start | bytes 3076
  292.5 47.1 %copy-start.18 = (f32[1,4,64]{2,1,0:T(4,128)S(1)}, f32[1,4,64]{2,1,0:T(4,128)}, u32[]{:S(2)}) copy-start(f32[1,4,64]{2,1,0:T(4,128)} %copy-done.17) | copy-start | bytes 3076
  292.5 47.1 %copy-start.20 = (f32[1,4,64]{2,1,0:T(4,128)S(1)}, f32[1,4,64]{2,1,0:T(4,128)}, u32[]{:S(2)}) copy-start(f32[1,4,64]{2,1,0:T(4,128)} %copy-done.19) | copy-start | bytes 3076
  292.5 47.3 %copy-start.24 = (f32[1,128]{1,0:T(1,128)S(1)}, f32[1,128]{1,0:T(1,128)}, u32[]{:S(2)}) copy-start(f32[1,128]{1,0:T(1,128)} %copy-done.23) | copy-start | bytes 1540
  292.5 47.3 %copy-start.27 = (f32[128]{0:T(128)S(1)}, f32[128]{0:T(128)}, u32[]{:S(2)}) copy-start(f32[128]{0:T(128)} %copy-done.26) | copy-start | bytes 1540
  292.5 47.5 %copy-start.12 = (bf16[128,512]{1,0:T(8,128)(2,1)S(1)}, bf16[128,512]{1,0:T(8,128)(2,1)}, u32[]{:S(2)}) copy-start(bf16[128,512]{1,0:T(8,128)(2,1)} %param.17) | copy-start | bytes 393220
  314.3 26.5 %copy-start.5 = (bf16[64,2048]{1,0:T(8,128)(2,1)S(1)}, bf16[64,2048]{1,0:T(8,128)(2,1)}, u32[]{:S(2)}) copy-start(bf16[64,2048]{1,0:T(8,128)(2,1)} %param.23) | copy-start | bytes 786436
  314.4 26.5 %copy-start.21 = (bf16[128,64]{0,1:T(8,128)(2,1)S(1)}, bf16[128,64]{0,1:T(8,128)(2,1)}, u32[]{:S(2)}) copy-start(bf16[128,64]{0,1:T(8,128)(2,1)} %param.20) | copy-start | bytes 49156
  342.1 33.2 %all-to-all-start = ((bf16[16,8,2048]{2,1,0:T(8,128)(2,1)}), bf16[16,8,2048]{2,1,0:T(8,128)(2,1)S(1)}, u32[]{:S(2)}, u32[]{:S(2)}) async-start(bf16[16,8,2048]{2,1,0:T(8,128)(2,1)} %fusion), calls=%async_computation | async-start | bytes 1048576 | tf_op jit(solution)/shard_map/all_to_all | solution.py:64
  376.4 41.6 %all-to-all-start.3 = ((bf16[16,16,2048]{2,1,0:T(8,128)(2,1)}), bf16[16,16,2048]{2,1,0:T(8,128)(2,1)S(1)}, u32[]{:S(2)}, u32[]{:S(2)}) async-start(bf16[16,16,2048]{2,1,0:T(8,128)(2,1)} %broadcast_in_dim.93), calls=%async_computation.4 | async-start | bytes 2097152 | tf_op jit(solution)/shard_map/all_to_all | solution.py:70
  (3 other events, 1.8 us)
Sparse Core Ops, SparseCore 0:
  292.6 61.3 reduce-scatter.1
where the time goes:
time: 428 us; the launch traced here: 427 us
  blocking collectives  186 us (43%)
  waiting for transfers between devices  64.6 us (15%)
  local copies, waits for them, and re-layouts  54.5 us (13%)
  between operations  49.7 us (12%)
  other arithmetic  27.8 us (6%)
  starting transfers between devices  26.2 us (6%)
  matrix products  17.5 us (4%)
    all_to_all x1, blocking collectives, expert_half(): lax.all_to_all(outgoing, EP, split_axis=0, concat_axis=0, tiled=True)  107 us
    all_to_all x1, waiting for transfers between devices, expert_half(): lax.all_to_all(partial_value, EP, split_axis=0, concat_axis=0, tiled=True)  48.3 us
    all_gather x2, blocking collectives, all_in_one(): both, at, found = (lax.all_gather(jnp.concatenate(lines), axis), 0, {})  41.1 us
    all_gather x1, blocking collectives, shards(): mixer_out = lax.all_gather(mixer_piece, 'tp', axis=0, tiled=True)  37.9 us
    gather x4, local copies, waits for them, and re-layouts, expert_half(): flat_back[gather_at[:, pick_index]].astype(jnp.float32)  23.9 us
    another operation x3, other arithmetic  18.2 us
    all_to_all x1, waiting for transfers between devices, summed_on_arrival(): lax.all_to_all(blocks, axis, split_axis=0, concat_axis=0, tiled=True)  16.3 us
    all_to_all x1, starting transfers between devices, summed_on_arrival(): lax.all_to_all(blocks, axis, split_axis=0, concat_axis=0, tiled=True)  16 us
  transfers between devices with their start and end apart: 4, of which 2 were waited for; matrix products, arithmetic and copies ran while one was open for 4% of the time, Pallas kernels for 0%

commit v1 on v0

--- a/solution.py
+++ b/solution.py
@@ -291,7 +291,8 @@
     mixer_piece = summed_on_arrival(mixer_partial.astype(jnp.bfloat16), "tp", 0).astype(
         jnp.bfloat16
     )
-    mixer_out = lax.all_gather(mixer_piece, "tp", axis=0, tiled=True)
+    sent = jnp.stack([mixer_piece] * lax.axis_size("tp"))
+    mixer_out = jnp.concatenate(lax.all_to_all(sent, "tp", 0, 0), axis=0)
     expert_piece = lax.psum_scatter(expert_partial, "tp", scatter_dimension=0, tiled=True).astype(
         jnp.bfloat16
     )

time: 428 us -> 462 us (1.079)
  blocking collectives: 186 us -> 228 us
  starting transfers between devices: 26.2 us -> 18.9 us
    all_to_all x1, waiting for transfers between devices: 48.3 us -> 0.01 us  [expert_half(): lax.all_to_all(partial_value, EP, split_axis=0, concat_axis=0, tiled=True)]
    all_gather x2, blocking collectives: 41.1 us -> 88 us  [all_in_one(): both, at, found = (lax.all_gather(jnp.concatenate(lines), axis), 0, {})]
    all_gather x1 -> x0, blocking collectives: 37.9 us -> none  [shards(): mixer_out = lax.all_gather(mixer_piece, 'tp', axis=0, tiled=True)]
    reduce_scatter x1, waiting for transfers between devices: 0.01 us -> 34.1 us  [shards(): lax.psum_scatter(expert_partial, 'tp', scatter_dimension=0, tiled=True)]
    all_to_all x0 -> x1, blocking collectives: none -> 33 us  [summed_on_arrival(): lax.all_to_all(blocks, axis, split_axis=0, concat_axis=0, tiled=True)]
    all_to_all x1, waiting for transfers between devices: 0.01 us -> 28 us  [from_everyone(): return lax.all_to_all(copies, axis, split_axis=0, concat_axis=0, tiled=True)]
    all_to_all x1, waiting for transfers between devices: 16.3 us -> 0.01 us  [shards(): mixer_out = jnp.concatenate(lax.all_to_all(sent, 'tp', 0, 0), axis=0)]
    all_to_all x1, starting transfers between devices: 16 us -> 3.47 us  [shards(): mixer_out = jnp.concatenate(lax.all_to_all(sent, 'tp', 0, 0), axis=0)]
where the time goes in v1:
time: 462 us; the launch traced here: 461 us
  blocking collectives  228 us (49%)
  waiting for transfers between devices  62.2 us (13%)
  local copies, waits for them, and re-layouts  55.8 us (12%)
  between operations  49.2 us (11%)
  other arithmetic  28.5 us (6%)
  starting transfers between devices  18.9 us (4%)
  matrix products  18.3 us (4%)
    all_to_all x1, blocking collectives, expert_half(): lax.all_to_all(outgoing, EP, split_axis=0, concat_axis=0, tiled=True)  107 us
    all_gather x2, blocking collectives, all_in_one(): both, at, found = (lax.all_gather(jnp.concatenate(lines), axis), 0, {})  88 us
    reduce_scatter x1, waiting for transfers between devices, shards(): lax.psum_scatter(expert_partial, 'tp', scatter_dimension=0, tiled=True)  34.1 us
    all_to_all x1, blocking collectives, summed_on_arrival(): lax.all_to_all(blocks, axis, split_axis=0, concat_axis=0, tiled=True)  33 us
    all_to_all x1, waiting for transfers between devices, from_everyone(): return lax.all_to_all(copies, axis, split_axis=0, concat_axis=0, tiled=True)  28 us
    gather x4, local copies, waits for them, and re-layouts, expert_half(): flat_back[gather_at[:, pick_index]].astype(jnp.float32)  23.9 us
    another operation x3, other arithmetic  18.2 us
  transfers between devices with their start and end apart: 4, of which 2 were waited for; matrix products, arithmetic and copies ran while one was open for 4% of the time, Pallas kernels for 0%

profile of v1, /device:TPU:1, one launch (start us, length us, event | category | flops | bytes accessed | tf_op | source)
XLA Modules:
  0.0 461.1 jit_solution(662745493397098917)
XLA Ops:
  7.2 0.9 copy.108
  8.6 18.0 %reduce-window.6 = s32[64,8,128]{2,1,0:T(8,128)S(1)} reduce-window(s32[64,8,128]{2,1,0:T(8,128)S(1)} %fusion.29, s32[]{:T(128)} %constant.140.clone.1), window={size=1x1x128 pad=0_0x0_0x127_0}, to_apply=%region_8.9 | reduce-window | flops 8323072 | bytes 524292 | tf_op jit(solution)/shard_map/reduce-window
  27.3 4.3 scatter_custom_fusion.1
  31.9 4.3 scatter_custom_fusion
  36.6 6.0 %gather_fusion = bf16[1024,2048]{1,0:T(8,128)(2,1)} fusion(bf16[256,2048]{1,0:T(8,128)(2,1)S(1)} %fusion.3, s32[1024]{0:T(1024)S(1)} %fusion.157), kind=kCustom, calls=%fused_computation | custom fusion | bytes 8392704 | tf_op jit(solution)/shard_map/gather | solution.py:227
  42.7 2.5 broadcast_select_fusion
  45.2 107.2 %all_to_all.25 = bf16[32,32,2048]{2,1,0:T(8,128)(2,1)S(1)} all-to-all(bf16[32,32,2048]{2,1,0:T(8,128)(2,1)S(1)} %broadcast_select_fusion), channel_id=1, replica_groups=mesh['ep_0'=8,'ep_1'=4,'tp'=16] {'ep_0','ep_1'}, dimensions={0} | all-to-all | bytes 8388608 | tf_op jit(solution)/shard_map/all_to_all | solution.py:232
  152.5 1.9 copy-done.1
  154.4 1.2 fusion.18
  155.7 8.5 %convolution_convert_fusion = bf16[32,32,2048]{2,1,0:T(8,128)(2,1)} fusion(bf16[32,32,2048]{2,1,0:T(8,128)(2,1)} %copy-done.1, bf16[1,128,2048]{2,1,0:T(8,128)(2,1)S(1)} %copy-done, bf16[1,2048,128]{2,1,0:T(8,128)(2,1)S(1)} %copy-done.5, f32[32,32,128]{2,1,0:T(8,128)S(1)} %fusion.18), kind=kOutput, calls=%fused_computation.8 | convolution fusion | flops 1076625408 | bytes 9961472 | tf_op jit(solution)/shard_map/sif,fd->sid/dot_general | solution.py:236
  164.2 6.7 %all-to-all-start.3 = ((bf16[32,32,2048]{2,1,0:T(8,128)(2,1)}), bf16[32,32,2048]{2,1,0:T(8,128)(2,1)}, u32[]{:S(2)}, u32[]{:S(2)}) async-start(bf16[32,32,2048]{2,1,0:T(8,128)(2,1)} %convolution_convert_fusion), calls=%async_computation.3 | async-start | bytes 8388608 | tf_op jit(solution)/shard_map/all_to_all | solution.py:240
  172.7 1.2 fusion.178
  175.3 1.3 subtract_exponential_fusion.1
  178.2 20.0 %all-gather.2 = f32[4,262,64]{1,2,0:T(8,128)S(1)} all-gather(f32[1,262,64]{1,2,0:T(8,128)S(1)} %maximum_bitcast_fusion), channel_id=2, replica_groups=mesh['ep_0'=8,'ep_1'=4,'tp'=16] {'ep_1'}, dimensions={0}, use_global_device_ids=true | all-gather | bytes 335360 | tf_op jit(solution)/shard_map/all_gather | solution.py:33
  210.6 68.0 %all-gather.3 = f32[8,262,64]{1,2,0:T(8,128)S(1)} all-gather(f32[1,262,64]{1,2,0:T(8,128)S(1)} %maximum_bitcast_fusion.1), channel_id=3, replica_groups=mesh['ep_0'=8,'ep_1'=4,'tp'=16] {'ep_0'}, dimensions={0}, use_global_device_ids=true | all-gather | bytes 603648 | tf_op jit(solution)/shard_map/all_gather | solution.py:33
  279.5 1.6 fusion.184
  307.3 0.9 slice_reduce_fusion.3
  308.2 1.0 fusion.188
  309.2 5.2 %gather_fusion.1 = bf16[256,2048]{1,0:T(8,128)(2,1)S(1)} fusion(bf16[1024,2048]{1,0:T(8,128)(2,1)} %bitcast.59, s32[1024]{0:T(1024)} %get-tuple-element.135), kind=kCustom, calls=%fused_computation.1 | custom fusion | bytes 2098176 | tf_op jit(solution)/shard_map/gather | solution.py:248
  314.4 6.2 %gather_fusion.2 = bf16[256,2048]{1,0:T(8,128)(2,1)} fusion(bf16[1024,2048]{1,0:T(8,128)(2,1)} %bitcast.59, s32[1024]{0:T(1024)} %get-tuple-element.134), kind=kCustom, calls=%fused_computation.2 | custom fusion | bytes 2098176 | tf_op jit(solution)/shard_map/gather | solution.py:248
  320.6 6.2 %gather_fusion.3 = bf16[256,2048]{1,0:T(8,128)(2,1)} fusion(bf16[1024,2048]{1,0:T(8,128)(2,1)} %bitcast.59, s32[1024]{0:T(1024)} %get-tuple-element.133), kind=kCustom, calls=%fused_computation.3 | custom fusion | bytes 2098176 | tf_op jit(solution)/shard_map/gather | solution.py:248
  326.9 6.2 %gather_fusion.4 = bf16[256,2048]{1,0:T(8,128)(2,1)} fusion(bf16[1024,2048]{1,0:T(8,128)(2,1)} %bitcast.59, s32[1024]{0:T(1024)} %get-tuple-element.132), kind=kCustom, calls=%fused_computation.4 | custom fusion | bytes 2098176 | tf_op jit(solution)/shard_map/gather | solution.py:248
  333.1 5.1 %convolution_add_fusion = f32[256,2048]{1,0:T(8,128)} fusion(bf16[32,2048]{1,0:T(8,128)(2,1)S(1)} %copy-done.9, bf16[256,2048]{1,0:T(8,128)(2,1)} %gather_fusion.4, bf16[256,2048]{1,0:T(8,128)(2,1)} %gather_fusion.3, bf16[256,2048]{1,0:T(8,128)(2,1)} %gather_fusion.2, bf16[256,2048]{1,0:T(8,128)(2,1)S(1)} %gather_fusion.1, bf16[256,2048]{1,0:T(8,128)(2,1)S(1)} %fusion.3, ...), kind=kOutput, calls=%fused_computation.9 | convolution fusion | flops 73449472 | bytes 7639040 | tf_op jit(solution)/shard_map/dot_general | solution.py:254
  340.3 1.3 convolution_multiply_fusion.4
  342.1 33.0 %all_to_all.26 = bf16[16,8,2048]{2,1,0:T(8,128)(2,1)S(1)} all-to-all(bf16[16,8,2048]{2,1,0:T(8,128)(2,1)S(1)} %fusion), channel_id=1, replica_groups=mesh['ep_0'=8,'ep_1'=4,'tp'=16] {'tp'}, dimensions={0} | all-to-all | bytes 1048576 | tf_op jit(solution)/shard_map/all_to_all | solution.py:64
  376.1 3.5 all-to-all-start.1
  379.6 34.1 %reduce-scatter.2.cloned.1.call-done = f32[16,2048]{1,0:T(8,128)} async-done(((f32[256,2048]{1,0:T(8,128)}), f32[16,2048]{1,0:T(8,128)}) %reduce-scatter.2.cloned.1.call-update) | async-done | bytes 131088 | tf_op jit(solution)/shard_map/reduce_scatter | solution.py:296
  413.7 0.9 convert_element_type.83
  414.6 1.1 broadcast_in_dim.93
  415.7 8.8 %all-to-all-start.4 = ((bf16[16,16,2048]{2,1,0:T(8,128)(2,1)}), bf16[16,16,2048]{2,1,0:T(8,128)(2,1)S(1)}, u32[]{:S(2)}, u32[]{:S(2)}) async-start(bf16[16,16,2048]{2,1,0:T(8,128)(2,1)} %broadcast_in_dim.93), calls=%async_computation.5 | async-start | bytes 2097152 | tf_op jit(solution)/shard_map/all_to_all | solution.py:70
  424.5 28.0 %all-to-all-done.4 = bf16[16,16,2048]{2,1,0:T(8,128)(2,1)S(1)} async-done(((bf16[16,16,2048]{2,1,0:T(8,128)(2,1)}), bf16[16,16,2048]{2,1,0:T(8,128)(2,1)S(1)}, u32[]{:S(2)}, u32[]{:S(2)}) %all-to-all-start.4) | async-done | bytes 1048608 | tf_op jit(solution)/shard_map/all_to_all | solution.py:70
  453.2 1.0 copy.150
  (152 shorter events, 15.5 us)
Async XLA Ops:
  7.2 148.5 %copy-start = (bf16[1,128,2048]{2,1,0:T(8,128)(2,1)S(1)}, bf16[1,128,2048]{2,1,0:T(8,128)(2,1)}, u32[]{:S(2)}) copy-start(bf16[1,128,2048]{2,1,0:T(8,128)(2,1)} %param.30) | copy-start | bytes 1572868
  7.2 24.4 %copy-start.2 = (bf16[256,2048]{1,0:T(8,128)(2,1)S(1)}, bf16[256,2048]{1,0:T(8,128)(2,1)}, u32[]{:S(2)}) copy-start(bf16[256,2048]{1,0:T(8,128)(2,1)} %param.24) | copy-start | bytes 3145732
  7.2 29.1 %copy-start.26 = (f32[2048]{0:T(1024)S(1)}, f32[2048]{0:T(1024)}, u32[]{:S(2)}) copy-start(f32[2048]{0:T(1024)} %param.25) | copy-start | bytes 24580
  45.2 109.2 %copy-start.4 = (bf16[1,2048,128]{2,1,0:T(8,128)(2,1)S(1)}, bf16[1,2048,128]{2,1,0:T(8,128)(2,1)}, u32[]{:S(2)}) copy-start(bf16[1,2048,128]{2,1,0:T(8,128)(2,1)} %param.28) | copy-start | bytes 1572868
  152.5 1.9 copy-start.1
  154.4 1.3 copy-start.5
  164.2 6.9 %copy-start.29 = (f32[128,2]{0,1:T(2,128)S(1)}, f32[128,2]{0,1:T(2,128)}, u32[]{:S(2)}) copy-start(f32[128,2]{0,1:T(2,128)} %param.21) | copy-start | bytes 3076
  164.2 6.9 %copy-start.30 = (f32[128,2]{0,1:T(2,128)S(1)}, f32[128,2]{0,1:T(2,128)}, u32[]{:S(2)}) copy-start(f32[128,2]{0,1:T(2,128)} %param.22) | copy-start | bytes 3076
  164.2 12.5 %copy-start.11 = (bf16[128,512]{1,0:T(8,128)(2,1)S(1)}, bf16[128,512]{1,0:T(8,128)(2,1)}, u32[]{:S(2)}) copy-start(bf16[128,512]{1,0:T(8,128)(2,1)} %param.18) | copy-start | bytes 393220
  164.2 13.7 %copy-start.13 = (bf16[128,64]{0,1:T(8,128)(2,1)S(1)}, bf16[128,64]{0,1:T(8,128)(2,1)}, u32[]{:S(2)}) copy-start(bf16[128,64]{0,1:T(8,128)(2,1)} %param.19) | copy-start | bytes 49156
  164.2 145.0 %all-to-all-start.3 = ((bf16[32,32,2048]{2,1,0:T(8,128)(2,1)}), bf16[32,32,2048]{2,1,0:T(8,128)(2,1)}, u32[]{:S(2)}, u32[]{:S(2)}) async-start(bf16[32,32,2048]{2,1,0:T(8,128)(2,1)} %convolution_convert_fusion), calls=%async_computation.3 | async-start | bytes 8388608 | tf_op jit(solution)/shard_map/all_to_all | solution.py:240
  170.8 242.9 %reduce-scatter.2.cloned.1.call-start = ((), (), s32[]{:S(2)}) async-start(), calls=%async_computation.6 | async-start | bytes 2228224 | tf_op jit(solution)/shard_map/reduce_scatter | solution.py:296
  171.1 5.6 %copy-start.27 = (f32[128]{0:T(128)}, f32[128]{0:T(128)S(1)}, u32[]{:S(2)}) copy-start(f32[128]{0:T(128)S(1)} %get-tuple-element.69) | copy-start | bytes 1540
  171.5 6.3 %copy-start.24 = (f32[1,128]{1,0:T(1,128)}, f32[1,128]{1,0:T(1,128)S(1)}, u32[]{:S(2)}) copy-start(f32[1,128]{1,0:T(1,128)S(1)} %reduce_window_sum.26) | copy-start | bytes 1540
  198.2 102.5 %copy-start.3 = (f32[4,262,64]{1,2,0:T(8,128)}, f32[4,262,64]{1,2,0:T(8,128)S(1)}, u32[]{:S(2)}) copy-start(f32[4,262,64]{1,2,0:T(8,128)S(1)} %all-gather.2) | copy-start | bytes 804868
  208.1 1.7 copy-start.15
  208.2 1.6 copy-start.17
  208.3 1.5 copy-start.19
  208.4 1.5 copy-start.21
  279.5 28.6 %copy-start.10 = (bf16[2048,32]{0,1:T(8,128)(2,1)S(1)}, bf16[2048,32]{0,1:T(8,128)(2,1)}, u32[]{:S(2)}) copy-start(bf16[2048,32]{0,1:T(8,128)(2,1)} %param.31) | copy-start | bytes 393220
  326.9 6.2 %copy-start.9 = (bf16[32,2048]{1,0:T(8,128)(2,1)S(1)}, bf16[32,2048]{1,0:T(8,128)(2,1)}, u32[]{:S(2)}) copy-start(bf16[32,2048]{1,0:T(8,128)(2,1)} %param.33) | copy-start | bytes 393220
  338.2 1.3 copy-start.20
  338.2 1.3 copy-start.22
  338.2 1.5 copy-start.25
  338.2 1.5 copy-start.28
  338.2 1.7 copy-start.12
  338.2 1.7 copy-start.14
  338.3 2.0 copy-start.8
  338.3 3.4 copy-start.6
  338.3 3.4 copy-start.23
  376.1 38.5 %all-to-all-start.1 = ((bf16[16,8,2048]{2,1,0:T(8,128)(2,1)}), bf16[16,8,2048]{2,1,0:T(8,128)(2,1)S(1)}, u32[]{:S(2)}, u32[]{:S(2)}) async-start(bf16[16,8,2048]{2,1,0:T(8,128)(2,1)} %stack.2), calls=%async_computation.1 | async-start | bytes 1048576 | tf_op jit(solution)/shard_map/all_to_all | solution.py:295
  415.7 36.7 %all-to-all-start.4 = ((bf16[16,16,2048]{2,1,0:T(8,128)(2,1)}), bf16[16,16,2048]{2,1,0:T(8,128)(2,1)S(1)}, u32[]{:S(2)}, u32[]{:S(2)}) async-start(bf16[16,16,2048]{2,1,0:T(8,128)(2,1)} %broadcast_in_dim.93), calls=%async_computation.5 | async-start | bytes 2097152 | tf_op jit(solution)/shard_map/all_to_all | solution.py:70
  (3 other events, 3.1 us)
Sparse Core Ops, SparseCore 0:
  338.4 75.2 reduce-scatter.1
